TPU v7x, 32 devices: a whole 2x2x4 slice. The times are simulated.
32 devices in a mesh: sp: 4 (over y, x), tp: 8 (over z, core).
Axes of the slice: x: 2, y: 2, z: 4, core: 2. Of those that a mesh axis runs over, the one named last changes fastest.
Arguments:
- tokens: bfloat16 [3, 2048, 4096], P(None, 'sp', 'tp'), may hold values from -6 to 6
- new_token: bfloat16 [3, 1, 4096], P(None, None, 'tp'), may hold values from -6 to 6
- query_weight: bfloat16 [4096, 4096], P(None, 'tp'), may hold values from -0.09375 to 0.09375
- key_weight: bfloat16 [4096, 4096], P(None, 'tp'), may hold values from -0.09375 to 0.09375
- value_weight: bfloat16 [4096, 4096], P(None, 'tp'), may hold values from -0.09375 to 0.09375
- log_decay: float32 [64], P('tp'), may hold values from -0.034 to 0
Outputs:
- state: bfloat16 [3, 64, 64, 64], P(None, 'tp', 'sp')
- read: bfloat16 [3, 4096], P(None, 'tp')
All inputs are finite; a program needn't handle non-finite values.
Results may differ from a plain program's by a relative error of at most 0.012.
Values may be sent and summed in bfloat16 or wider, within the bound.
A program may use at most 64 MiB of HBM per device.

v0:
```python
import jax
import jax.numpy as jnp
from jax import lax
from jax.sharding import PartitionSpec as P

HD = 64


def rotate(values, positions):
    half_dim = values.shape[-1] // 2
    inverse = 10000.0 ** (-jnp.arange(half_dim, dtype=jnp.float32) / half_dim)
    angles = positions.astype(jnp.float32)[:, None, None] * inverse[None, None, :]
    cosine = jnp.cos(angles)
    sine_part = jnp.sin(angles)
    first = values[..., :half_dim]
    second = values[..., half_dim:]
    return jnp.concatenate(
        [first * cosine - second * sine_part, first * sine_part + second * cosine], axis=-1
    )


def group_norm(output):
    centered = output - jnp.mean(output, axis=-1, keepdims=True)
    return centered * lax.rsqrt(jnp.mean(centered * centered, axis=-1, keepdims=True) + 1e-05)


def body(tokens, new_token, query_weight, key_weight, value_weight, log_decay):
    sequences, span_len, _ = tokens.shape
    head_count = log_decay.shape[0]
    inner = head_count * HD
    groups = lax.axis_size("sp")
    own_index = lax.axis_index("sp")
    key_scale = HD ** (-0.5)
    key_share = HD // groups
    row_weights = jnp.concatenate([key_weight, value_weight], axis=1)
    all_weights = jnp.concatenate([key_weight, value_weight, query_weight], axis=1)
    row_piece = lax.all_gather(tokens, "tp", axis=2, tiled=True)
    new_piece = lax.all_gather(new_token, "tp", axis=2, tiled=True)
    row_total = jnp.dot(row_piece, row_weights, preferred_element_type=jnp.float32)
    new_total = jnp.dot(new_piece, all_weights, preferred_element_type=jnp.float32)
    row_total = row_total.reshape(sequences, span_len, 2, head_count, HD)
    offsets = own_index * span_len + jnp.arange(span_len, dtype=jnp.int32)
    key_rows = (rotate(row_total[:, :, 0], offsets) * key_scale).astype(jnp.bfloat16)
    value_rows = row_total[:, :, 1].astype(jnp.bfloat16)
    to_end = (span_len - 1 - jnp.arange(span_len, dtype=jnp.int32)).astype(jnp.float32)
    decay_rows = jnp.exp(to_end[:, None] * log_decay[None, :])
    weighted = (key_rows.astype(jnp.float32) * decay_rows[None, :, :, None]).astype(jnp.bfloat16)
    span_state = jnp.einsum(
        "sthk,sthv->shkv", weighted, value_rows, preferred_element_type=jnp.float32
    )
    carried_state = jnp.exp(log_decay * (span_len * (groups - 1 - own_index)).astype(jnp.float32))
    scaled_state = span_state * carried_state[None, :, None, None]
    state_rows = lax.psum_scatter(scaled_state, "sp", scatter_dimension=2, tiled=True)
    new_total = new_total.reshape(sequences, 1, 3, head_count, HD)
    new_position = jnp.full((1,), groups * span_len, jnp.int32)
    fresh_key = (rotate(new_total[:, :, 0], new_position) * key_scale).astype(jnp.bfloat16)[:, 0]
    new_value = new_total[:, 0, 1].astype(jnp.bfloat16)
    new_query = rotate(new_total[:, :, 2], new_position).astype(jnp.bfloat16)[:, 0]
    query_entries = new_query.astype(jnp.float32)
    decay_one = jnp.exp(log_decay)[None, :, None]
    query_share = lax.dynamic_slice_in_dim(query_entries, own_index * key_share, key_share, 2)
    partial_read = (
        jnp.einsum("shkv,shk->shv", state_rows, query_share, precision=lax.Precision.HIGHEST)
        * decay_one
    )
    summed = lax.psum(partial_read, "sp")
    own_term = jnp.sum(
        query_entries * fresh_key.astype(jnp.float32), axis=-1, keepdims=True
    ) * new_value.astype(jnp.float32)
    normed = group_norm(summed + own_term)
    return (state_rows.astype(jnp.bfloat16), normed.reshape(sequences, inner).astype(jnp.bfloat16))


def solution(mesh):
    return jax.shard_map(
        body,
        mesh=mesh,
        in_specs=(
            P(None, "sp", "tp"),
            P(None, None, "tp"),
            P(None, "tp"),
            P(None, "tp"),
            P(None, "tp"),
            P("tp"),
        ),
        out_specs=(P(None, "tp", "sp", None), P(None, "tp")),
        check_vma=False,
    )
```

profile of v0, /device:TPU:0, one launch (start us, length us, event | category | flops | bytes accessed | tf_op | source)
XLA Modules:
  0.0 200.9 jit_solution(10623617118696532471)
XLA Ops:
  7.2 0.0 all-gather.2.cloned.1.call-start
  7.2 0.7 all-gather.2.cloned.1.call-update
  7.9 0.0 reduce-scatter.2.cloned.1.call-start
  7.9 6.4 %copy.9 = bf16[4096,512]{0,1:T(8,128)(2,1)} copy(bf16[4096,512]{1,0:T(8,128)(2,1)} %param.10) | data formatting | bytes 8388608 | tf_op args[4]
  14.3 0.0 copy-start
  14.3 0.0 copy-start.1
  14.3 6.5 %copy.8 = bf16[4096,512]{0,1:T(8,128)(2,1)} copy(bf16[4096,512]{1,0:T(8,128)(2,1)} %param.9) | data formatting | bytes 8388608 | tf_op args[3]
  20.8 0.0 copy-done
  20.8 16.8 %all_gather.7 = bf16[3,1,4096]{2,0,1:T(4,128)(2,1)S(1)} all-gather(bf16[3,1,512]{2,0,1:T(4,128)(2,1)S(1)} %copy-done), channel_id=1, replica_groups=mesh['sp'=4,'tp'=8] {'tp'}, dimensions={2}, use_global_device_ids=true | all-gather | bytes 27648 | tf_op jit(solution)/shard_map/all_gather | solution.py:38
  37.7 0.0 copy-done.1
  37.7 0.1 multiply_exponential_fusion
  37.8 0.3 multiply_cosine_fusion
  38.1 91.1 %all-gather.2.cloned.1.call-done = bf16[3,512,4096]{2,1,0:T(8,128)(2,1)} async-done(((bf16[3,512,512]{2,1,0:T(8,128)(2,1)}), bf16[3,512,4096]{2,1,0:T(8,128)(2,1)}) %all-gather.2.cloned.1.call-update) | async-done | bytes 12582928 | tf_op jit(solution)/shard_map/all_gather | solution.py:37
  129.3 18.5 %fusion.7 = f32[1024,3,512]{2,0,1:T(8,128)S(1)} fusion(bf16[3,512,4096]{2,1,0:T(8,128)(2,1)} %all-gather.2.cloned.1.call-done, bf16[4096,512]{0,1:T(8,128)(2,1)} %copy.9, bf16[4096,512]{0,1:T(8,128)(2,1)} %copy.8), kind=kOutput, calls=%fused_computation.8 | convolution fusion | flops 12901679104 | bytes 27262976 | tf_op jit(solution)/shard_map/dot_general | solution.py:39
  147.8 0.3 copy_bitcast_fusion
  148.1 0.5 multiply_subtract_fusion
  148.5 1.5 fusion.20
  150.0 0.0 reduce-scatter.2.cloned.1.call-update
  150.0 5.6 %fusion.11 = f32[3,1536]{1,0:T(4,128)S(1)} fusion(bf16[4096,512]{1,0:T(8,128)(2,1)} %param.8, bf16[4096,512]{1,0:T(8,128)(2,1)} %param.10, bf16[4096,512]{1,0:T(8,128)(2,1)} %param.9, bf16[3,1,4096]{2,0,1:T(4,128)(2,1)S(1)} %all_gather.7), kind=kOutput, calls=%fused_computation.16 | convolution fusion | flops 75497472 | bytes 12625920 | tf_op jit(solution)/shard_map/dot_general | solution.py:40
  155.6 0.1 reshape.216
  155.7 0.1 multiply_sine_fusion.1
  155.8 0.1 subtract_bitcast_fusion
  155.8 0.1 fusion.31
  155.9 18.7 %reduce-scatter.2.cloned.1.call-done = f32[3,8,16,64]{3,2,1,0:T(8,128)} async-done(((f32[3,8,64,64]{3,2,1,0:T(8,128)}), f32[3,8,16,64]{3,2,1,0:T(8,128)}) %reduce-scatter.2.cloned.1.call-update) | async-done | bytes 98320 | tf_op jit(solution)/shard_map/reduce_scatter | solution.py:53
  174.6 1.1 fusion.27
  175.7 0.1 broadcast_multiply_fusion
  175.8 15.0 %psum.7 = f32[3,8,64]{2,1,0:T(8,128)S(1)} all-reduce(f32[3,8,64]{2,1,0:T(8,128)S(1)} %broadcast_multiply_fusion), channel_id=1, replica_groups=mesh['sp'=4,'tp'=8] {'sp'}, use_global_device_ids=true, to_apply=%region_1.0 | all-reduce | flops 1536 | bytes 12288 | tf_op jit(solution)/shard_map/psum | solution.py:66
  190.8 0.7 fusion.38
  191.6 0.2 multiply_reduce_fusion
  191.7 0.1 multiply_convert_fusion.4
  191.8 0.7 convert_element_type.83
  192.5 1.6 convert_element_type.76
  (7 shorter events, 0.0 us)
Async XLA Ops:
  7.2 122.1 %all-gather.2.cloned.1.call-start = ((), (), s32[]{:S(2)}) async-start(), calls=%async_computation.1 | async-start | bytes 14155776 | tf_op jit(solution)/shard_map/all_gather | solution.py:37
  7.9 166.7 %reduce-scatter.2.cloned.1.call-start = ((), (), s32[]{:S(2)}) async-start(), calls=%async_computation.2 | async-start | bytes 983040 | tf_op jit(solution)/shard_map/reduce_scatter | solution.py:53
  14.3 6.5 %copy-start = (bf16[3,1,512]{2,0,1:T(4,128)(2,1)S(1)}, bf16[3,1,512]{2,0,1:T(4,128)(2,1)}, u32[]{:S(2)}) copy-start(bf16[3,1,512]{2,0,1:T(4,128)(2,1)} %param.7) | copy-start | bytes 9220
  14.3 23.4 %copy-start.1 = (f32[8]{0:T(128)S(1)}, f32[8]{0:T(128)}, u32[]{:S(2)}) copy-start(f32[8]{0:T(128)} %param.11) | copy-start | bytes 100
Sparse Core Ops, SparseCore 0:
  9.6 119.6 all-gather.1
  150.1 24.4 reduce-scatter.1
where the time goes:
time: 201 us
  waiting for transfers between devices  110 us (55%)
  blocking collectives  31.9 us (16%)
  matrix products  26.7 us (13%)
  between operations  14.1 us (7%)
  local copies, waits for them, and re-layouts  14 us (7%)
  other arithmetic  3.69 us (2%)
    all_gather x1, waiting for transfers between devices, body(): row_piece = lax.all_gather(tokens, 'tp', axis=2, tiled=True)  91.1 us
    reduce_scatter x1, waiting for transfers between devices, body(): lax.psum_scatter(scaled_state, 'sp', scatter_dimension=2, tiled=True)  18.7 us
    dot_general x1, matrix products, body(): jnp.dot(row_piece, row_weights, preferred_element_type=jnp.float32)  18.5 us
    all_gather x1, blocking collectives, body(): new_piece = lax.all_gather(new_token, 'tp', axis=2, tiled=True)  16.8 us
    psum x1, blocking collectives, body(): summed = lax.psum(partial_read, 'sp')  15 us
    unnamed x6, local copies, waits for them, and re-layouts  12.9 us
    dot_general x1, matrix products, body(): jnp.dot(new_piece, all_weights, preferred_element_type=jnp.float32)  5.59 us
  transfers between devices with their start and end apart: 2, of which 2 were waited for; matrix products, arithmetic and copies ran while one was open for 10% of the time, Pallas kernels for 0%

commit v1 on v0

--- a/solution.py
+++ b/solution.py
@@ -63,7 +63,7 @@
         jnp.einsum("shkv,shk->shv", state_rows, query_share, precision=lax.Precision.HIGHEST)
         * decay_one
     )
-    summed = lax.psum(partial_read, "sp")
+    summed = jnp.sum(lax.all_gather(partial_read, "sp"), axis=0)
     own_term = jnp.sum(
         query_entries * fresh_key.astype(jnp.float32), axis=-1, keepdims=True
     ) * new_value.astype(jnp.float32)

time: 201 us -> 194 us (0.965)
  blocking collectives: 31.9 us -> 25.1 us
    psum x1 -> x0, blocking collectives: 15 us -> none  [body(): summed = lax.psum(partial_read, 'sp')]
    all_gather x0 -> x1, blocking collectives: none -> 8.26 us  [body(): summed = jnp.sum(lax.all_gather(partial_read, 'sp'), axis=0)]
    all_gather x1, waiting for transfers between devices: 91.1 us -> 85.3 us  [body(): row_piece = lax.all_gather(tokens, 'tp', axis=2, tiled=True)]
    reduce_scatter x1, waiting for transfers between devices: 18.7 us -> 23.9 us  [body(): lax.psum_scatter(scaled_state, 'sp', scatter_dimension=2, tiled=True)]
where the time goes in v1:
time: 194 us
  waiting for transfers between devices  110 us (57%)
  matrix products  26.8 us (14%)
  blocking collectives  25.1 us (13%)
  between operations  14.1 us (7%)
  local copies, waits for them, and re-layouts  13.9 us (7%)
  other arithmetic  3.86 us (2%)
    all_gather x1, waiting for transfers between devices, body(): row_piece = lax.all_gather(tokens, 'tp', axis=2, tiled=True)  85.3 us
    reduce_scatter x1, waiting for transfers between devices, body(): lax.psum_scatter(scaled_state, 'sp', scatter_dimension=2, tiled=True)  23.9 us
    dot_general x1, matrix products, body(): jnp.dot(row_piece, row_weights, preferred_element_type=jnp.float32)  18.5 us
    all_gather x1, blocking collectives, body(): new_piece = lax.all_gather(new_token, 'tp', axis=2, tiled=True)  16.8 us
    unnamed x6, local copies, waits for them, and re-layouts  12.9 us
    all_gather x1, blocking collectives, body(): summed = jnp.sum(lax.all_gather(partial_read, 'sp'), axis=0)  8.26 us
    dot_general x1, matrix products, body(): jnp.dot(new_piece, all_weights, preferred_element_type=jnp.float32)  5.7 us
  transfers between devices with their start and end apart: 2, of which 2 were waited for; matrix products, arithmetic and copies ran while one was open for 10% of the time, Pallas kernels for 0%

profile of v1, /device:TPU:0, one launch (start us, length us, event | category | flops | bytes accessed | tf_op | source)
XLA Modules:
  0.0 193.8 jit_solution(7615783362770031967)
XLA Ops:
  7.2 0.7 all-gather.3.cloned.1.call-update
  7.9 6.4 %copy.14 = bf16[4096,512]{0,1:T(8,128)(2,1)} copy(bf16[4096,512]{1,0:T(8,128)(2,1)} %param.10) | data formatting | bytes 8388608 | tf_op args[4]
  14.4 6.5 %copy.13 = bf16[4096,512]{0,1:T(8,128)(2,1)} copy(bf16[4096,512]{1,0:T(8,128)(2,1)} %param.9) | data formatting | bytes 8388608 | tf_op args[3]
  20.9 16.8 %all_gather.13 = bf16[3,1,4096]{2,0,1:T(4,128)(2,1)S(1)} all-gather(bf16[3,1,512]{2,0,1:T(4,128)(2,1)S(1)} %copy-done), channel_id=1, replica_groups=mesh['sp'=4,'tp'=8] {'tp'}, dimensions={2}, use_global_device_ids=true | all-gather | bytes 27648 | tf_op jit(solution)/shard_map/all_gather | solution.py:38
  37.7 5.7 %fusion.10 = f32[3,1536]{1,0:T(4,128)S(1)} fusion(bf16[4096,512]{1,0:T(8,128)(2,1)} %param.8, bf16[4096,512]{1,0:T(8,128)(2,1)} %param.10, bf16[4096,512]{1,0:T(8,128)(2,1)} %param.9, bf16[3,1,4096]{2,0,1:T(4,128)(2,1)S(1)} %all_gather.13), kind=kOutput, calls=%fused_computation.15 | convolution fusion | flops 75497472 | bytes 12625920 | tf_op jit(solution)/shard_map/dot_general | solution.py:40
  43.4 0.1 reshape.223
  43.6 0.1 multiply_exponential_fusion
  43.7 0.3 multiply_cosine_fusion
  44.0 85.3 %all-gather.3.cloned.1.call-done = bf16[3,512,4096]{2,1,0:T(8,128)(2,1)} async-done(((bf16[3,512,512]{2,1,0:T(8,128)(2,1)}), bf16[3,512,4096]{2,1,0:T(8,128)(2,1)}) %all-gather.3.cloned.1.call-update) | async-done | bytes 12582928 | tf_op jit(solution)/shard_map/all_gather | solution.py:37
  129.3 18.5 %fusion.6 = f32[1024,3,512]{2,0,1:T(8,128)S(1)} fusion(bf16[3,512,4096]{2,1,0:T(8,128)(2,1)} %all-gather.3.cloned.1.call-done, bf16[4096,512]{0,1:T(8,128)(2,1)} %copy.14, bf16[4096,512]{0,1:T(8,128)(2,1)} %copy.13), kind=kOutput, calls=%fused_computation.7 | convolution fusion | flops 12901679104 | bytes 27262976 | tf_op jit(solution)/shard_map/dot_general | solution.py:39
  147.8 0.3 copy_bitcast_fusion
  148.1 0.5 multiply_subtract_fusion
  148.5 1.5 fusion.19
  150.0 0.1 subtract_bitcast_fusion
  150.1 0.2 multiply_reduce_fusion.1
  150.3 0.1 mul.283
  150.3 0.1 mul.284
  150.4 0.1 reshape.224
  150.5 0.1 fusion.28
  150.6 23.9 %reduce-scatter.2.cloned.1.call-done = f32[3,8,16,64]{3,2,1,0:T(8,128)} async-done(((f32[3,8,64,64]{3,2,1,0:T(8,128)}), f32[3,8,16,64]{3,2,1,0:T(8,128)}) %reduce-scatter.2.cloned.1.call-update) | async-done | bytes 98320 | tf_op jit(solution)/shard_map/reduce_scatter | solution.py:53
  174.5 1.1 fusion.25
  175.7 0.1 broadcast_multiply_fusion
  175.7 8.3 %all-gather = f32[12,8,64]{2,1,0:T(8,128)S(1)} all-gather(f32[3,8,64]{2,1,0:T(8,128)S(1)} %broadcast_multiply_fusion), channel_id=2, replica_groups=mesh['sp'=4,'tp'=8] {'sp'}, dimensions={0}, use_global_device_ids=true | all-gather | bytes 30720 | tf_op jit(solution)/shard_map/all_gather | solution.py:66
  184.0 0.2 fusion.29
  184.2 0.1 reduce_sum.39
  184.2 0.2 multiply_reduce_fusion
  184.4 0.1 mul.288
  184.5 0.1 mul.289
  184.6 0.1 sub.41
  184.6 0.1 sub.42
  184.7 0.6 multiply_convert_fusion.4
  185.3 1.6 convert_element_type.83
  (17 shorter events, 0.2 us)
Async XLA Ops:
  7.2 122.1 %all-gather.3.cloned.1.call-start = ((), (), s32[]{:S(2)}) async-start(), calls=%async_computation.1 | async-start | bytes 14155776 | tf_op jit(solution)/shard_map/all_gather | solution.py:37
  7.9 166.6 %reduce-scatter.2.cloned.1.call-start = ((), (), s32[]{:S(2)}) async-start(), calls=%async_computation.2 | async-start | bytes 983040 | tf_op jit(solution)/shard_map/reduce_scatter | solution.py:53
  14.4 6.5 %copy-start = (bf16[3,1,512]{2,0,1:T(4,128)(2,1)S(1)}, bf16[3,1,512]{2,0,1:T(4,128)(2,1)}, u32[]{:S(2)}) copy-start(bf16[3,1,512]{2,0,1:T(4,128)(2,1)} %param.7) | copy-start | bytes 9220
  37.7 5.9 %copy-start.1 = (f32[8]{0:T(128)S(1)}, f32[8]{0:T(128)}, u32[]{:S(2)}) copy-start(f32[8]{0:T(128)} %param.11) | copy-start | bytes 100
Sparse Core Ops, SparseCore 0:
  9.6 119.6 all-gather.2
  150.1 24.3 reduce-scatter.1
